TPU v7x, 32 devices: a whole 2x2x4 slice. The times are simulated.
32 devices in a mesh: sp: 16 (over z, y, x), tp: 2 (over core).
Axes of the slice: x: 2, y: 2, z: 4, core: 2. Of those that a mesh axis runs over, the one named last changes fastest.
Arguments:
- queries: bfloat16 [4096, 1024], P('sp', 'tp'), may hold values from -6 to 6
- keys: bfloat16 [4096, 512], P('sp', 'tp'), may hold values from -6 to 6
- values: bfloat16 [4096, 512], P('sp', 'tp'), may hold values from -6 to 6
- q_gain: float32 [64], replicated, may hold values from 1.6 to 4.5
- key_norm_gain: float32 [64], replicated, may hold values from 1.6 to 4.5
- out_weight: bfloat16 [1024, 2048], P('tp'), may hold values from -0.1875 to 0.1875
- residual: bfloat16 [4096, 2048], P('sp'), may hold values from -6 to 6
- ln1_gain: float32 [2048], replicated, may hold values from 0.1 to 1.9
- ln1_bias: float32 [2048], replicated, may hold values from -3 to 3
- up_weight: bfloat16 [2048, 8192], P('sp', 'tp'), may hold values from -0.125 to 0.125
- down_weight: bfloat16 [8192, 2048], P('tp', 'sp'), may hold values from -0.0625 to 0.0625
- ln2_gain: float32 [2048], replicated, may hold values from 0.1 to 1.9
- ln2_bias: float32 [2048], replicated, may hold values from -3 to 3
Outputs:
- encoded: bfloat16 [4096, 2048], P('sp', 'tp')
All inputs are finite; a program needn't handle non-finite values.
Results may differ from a plain program's by a relative error of at most 0.014.
Values may be sent and summed in bfloat16 or wider, within the bound.
No kernel may reach another device: no remote copies, remote signals or barrier semaphores. Data moves between devices by JAX's collectives and lax.ppermute only.
A program may use at most 128 MiB of HBM per device.

v0:
```python
import math
import jax
import jax.numpy as jnp
from jax import lax
from jax.sharding import PartitionSpec as P

D = 2048
HEAD_SIZE = 64
GRID_W = 64
ALPHA = 8.0**0.25
ROTARY_BASE = 10000.0
RMS_EPSILON = 1e-06
NORM_EPSILON = 1e-05


def rotate_grid(heads_in, grid_places):
    half_dim = heads_in.shape[-1] // 2
    quarter = half_dim // 2
    inverse = ROTARY_BASE ** (-jnp.arange(quarter, dtype=jnp.float32) / quarter)

    def spin(segment, coords):
        angles = coords.astype(jnp.float32)[:, None] * inverse[None, :]
        cos_val = jnp.cos(angles)[:, None, :]
        sin_val = jnp.sin(angles)[:, None, :]
        lead_half = segment[..., :quarter]
        tail_half = segment[..., quarter:]
        return jnp.concatenate(
            [lead_half * cos_val - tail_half * sin_val, tail_half * cos_val + lead_half * sin_val],
            -1,
        )

    return jnp.concatenate(
        [
            spin(heads_in[..., :half_dim], grid_places // GRID_W),
            spin(heads_in[..., half_dim:], grid_places % GRID_W),
        ],
        -1,
    )


def prepare_inputs(heads_in, gain_vec, grid_places, factor):
    values32 = heads_in.astype(jnp.float32)
    normed = (
        values32
        * lax.rsqrt(jnp.mean(values32 * values32, -1, keepdims=True) + RMS_EPSILON)
        * gain_vec
    )
    return (rotate_grid(normed, grid_places) * factor).astype(jnp.bfloat16)


def layer_norm(pre_norm, gain_vec, bias_vec):
    row_mean = jnp.mean(pre_norm, -1, keepdims=True)
    centred = pre_norm - row_mean
    spread = jnp.mean(centred * centred, -1, keepdims=True)
    return centred * lax.rsqrt(spread + NORM_EPSILON) * gain_vec + bias_vec


def finish_norm(pre_norm, stats, gain_vec, bias_vec):
    row_mean = stats[0][:, None] / D
    spread = stats[1][:, None] / D - row_mean * row_mean
    return (pre_norm - row_mean) * lax.rsqrt(spread + NORM_EPSILON) * gain_vec + bias_vec


def take_cols(array_in, col_start, col_width):
    return lax.dynamic_slice_in_dim(array_in, col_start, col_width, array_in.ndim - 1)


def local(
    queries,
    keys,
    values,
    q_gain,
    key_norm_gain,
    out_weight,
    residual,
    ln1_gain,
    ln1_bias,
    up_weight,
    down_weight,
    ln2_gain,
    ln2_bias,
):
    tok_rows = queries.shape[0]
    grid_places = lax.axis_index("sp") * tok_rows + jnp.arange(tok_rows, dtype=jnp.int32)
    kv_heads = keys.shape[1] // HEAD_SIZE
    q_count = queries.shape[1] // HEAD_SIZE
    group_count_size = q_count // kv_heads
    query_head_rows = prepare_inputs(
        queries.reshape(tok_rows, q_count, HEAD_SIZE), q_gain, grid_places, HEAD_SIZE ** (-0.5)
    )
    q_grouped = query_head_rows.reshape(tok_rows, kv_heads, group_count_size, HEAD_SIZE)
    k_sent = prepare_inputs(
        keys.reshape(tok_rows, kv_heads, HEAD_SIZE), key_norm_gain, grid_places, 1.0
    ).reshape(tok_rows, kv_heads * HEAD_SIZE)
    initial = (
        jnp.full((kv_heads, group_count_size, tok_rows), -jnp.inf, jnp.float32),
        jnp.zeros((kv_heads, group_count_size, tok_rows), jnp.float32),
        jnp.zeros((tok_rows, kv_heads, group_count_size, HEAD_SIZE), jnp.float32),
    )
    key_piece = lax.all_gather(k_sent, "sp", axis=0, tiled=True)
    value_piece = lax.all_gather(values, "sp", axis=0, tiled=True)
    key_count = key_piece.shape[0]
    block_len = math.gcd(key_count, 2048)
    key_blocks = key_piece.reshape(key_count // block_len, block_len, kv_heads, HEAD_SIZE)
    value_blocks = value_piece.reshape(key_count // block_len, block_len, kv_heads, HEAD_SIZE)

    def advance(state_in, blocks):
        maxima, totals, accumulated = state_in
        scores = jnp.einsum(
            "qhgd,khd->hgqk", q_grouped, blocks[0], preferred_element_type=jnp.float32
        )
        new_max = jnp.maximum(maxima, jnp.max(scores, -1))
        factor = jnp.exp(maxima - new_max)
        weights = jnp.exp(scores - new_max[..., None])
        totals = totals * factor + jnp.sum(weights, -1)
        update = jnp.einsum(
            "hgqk,khd->qhgd",
            weights.astype(jnp.bfloat16),
            blocks[1],
            preferred_element_type=jnp.float32,
        )
        accumulated = accumulated * jnp.transpose(factor, (2, 0, 1))[..., None] + update
        return ((new_max, totals, accumulated), None)

    state_out, unused = lax.scan(advance, initial, (key_blocks, value_blocks))
    maxima, totals, accumulated = state_out
    attended = (
        (accumulated / jnp.transpose(totals, (2, 0, 1))[..., None])
        .reshape(tok_rows, q_count * HEAD_SIZE)
        .astype(jnp.bfloat16)
    )
    partial_value = jnp.dot(attended, out_weight, preferred_element_type=jnp.float32)
    col_width = D // lax.axis_size("tp")
    col_start = lax.axis_index("tp") * col_width
    mixed_sum = lax.psum(partial_value.astype(jnp.bfloat16), "tp").astype(jnp.float32)
    full_rows = layer_norm(
        ALPHA * residual.astype(jnp.float32) + mixed_sum, ln1_gain, ln1_bias
    ).astype(jnp.bfloat16)
    normed_own = take_cols(full_rows, col_start, col_width)
    up_acts = jnp.dot(
        full_rows,
        lax.all_gather(up_weight, "sp", axis=0, tiled=True),
        preferred_element_type=jnp.float32,
    )
    hidden = jnp.square(jnp.maximum(up_acts, 0.0)).astype(jnp.bfloat16)
    partial_ffn = jnp.dot(
        hidden,
        lax.all_gather(down_weight, "sp", axis=1, tiled=True),
        preferred_element_type=jnp.float32,
    )
    ffn_cols = lax.psum_scatter(
        partial_ffn.astype(jnp.bfloat16), "tp", scatter_dimension=1, tiled=True
    ).astype(jnp.float32)
    second = ALPHA * normed_own.astype(jnp.float32) + ffn_cols
    stats_two = lax.psum((jnp.sum(second, -1), jnp.sum(second * second, -1)), "tp")
    return finish_norm(
        second,
        stats_two,
        take_cols(ln2_gain, col_start, col_width),
        take_cols(ln2_bias, col_start, col_width),
    ).astype(jnp.bfloat16)


def solution(mesh):
    return jax.shard_map(
        local,
        mesh=mesh,
        in_specs=(
            P("sp", "tp"),
            P("sp", "tp"),
            P("sp", "tp"),
            P(),
            P(),
            P("tp", None),
            P("sp", None),
            P(),
            P(),
            P("sp", "tp"),
            P("tp", "sp"),
            P(),
            P(),
        ),
        out_specs=P("sp", "tp"),
        check_vma=False,
    )
```

profile of v0, /device:TPU:0, one launch (start us, length us, event | category | flops | bytes accessed | tf_op | source)
XLA Modules:
  0.0 704.4 jit_solution(7267192037591548552)
XLA Ops:
  6.6 1.1 copy.21
  7.8 0.7 fusion.30
  8.5 0.2 multiply_cosine_fusion.1
  8.8 0.7 pad_maximum_fusion
  9.4 0.0 all-gather.5.cloned.1.call-update
  9.5 0.0 all-gather.7.cloned.1.call-start
  9.5 0.7 all-gather.7.cloned.1.call-update
  10.2 0.0 all-reduce.3.cloned.1.call-start
  10.3 1.1 copy.22
  11.4 0.1 fusion.26
  11.5 0.0 copy-done.6
  11.5 0.1 fusion.27
  11.6 0.1 multiply_subtract_fusion.1
  11.7 65.8 %all-gather.5.cloned.1.call-done = bf16[4096,256]{0,1:T(8,128)(2,1)} async-done(((bf16[256,256]{0,1:T(8,128)(2,1)}), bf16[4096,256]{0,1:T(8,128)(2,1)}) %all-gather.5.cloned.1.call-update) | async-done | bytes 2097168 | tf_op jit(solution)/shard_map/all_gather | solution.py:100
  77.5 4.5 reshape.201
  82.0 3.8 copy.24
  85.8 53.3 %all-gather.7.cloned.1.call-done = bf16[4096,256]{1,0:T(8,128)(2,1)} async-done(((bf16[256,256]{1,0:T(8,128)(2,1)}), bf16[4096,256]{1,0:T(8,128)(2,1)}) %all-gather.7.cloned.1.call-update) | async-done | bytes 2097168 | tf_op jit(solution)/shard_map/all_gather | solution.py:101
  139.1 7.1 %reshape.207 = bf16[2,2048,4,64]{3,2,1,0:T(4,128)(2,1)} reshape(bf16[4096,256]{1,0:T(8,128)(2,1)} %all-gather.7.cloned.1.call-done) | data formatting | bytes 4194304 | tf_op jit(solution)/shard_map/reshape | solution.py:105
  146.2 6.9 copy.25
  153.1 49.9 %while.15 = (s32[]{:T(128)}, f32[4,2,256]{2,1,0:T(2,128)S(1)}, f32[4,2,256]{2,1,0:T(2,128)S(1)}, f32[256,4,2,64]{0,3,2,1:T(8,128)S(1)}, bf16[2,2048,4,64]{1,3,2,...) while((s32[]{:T(128)}, f32[4,2,256]{2,1,0:T(2,128)S(1)}, ...), condition=%wide.region_5.6_spmd.clone, body=%wide.region_2.5_spmd.clone.sunk | while | flops 1095118848 | bytes 53871716 | solution.py:125
  153.1 9.3 %bitcast_reduce_fusion.2 = (f32[4,2,256]{2,1,0:T(2,128)S(1)}, f32[4,2048,256,2]{2,1,3,0:T(8,128)}) fusion(bf16[256,4,2,64]{0,3,2,1:T(8,128)(2,1)S(1)} %get-tuple-element.194, bf16[2,2048,4,64]{1,3,2,0:T(8,128)(2,1)} %get-tuple-element.193, s32[]{:T(128)} %get-tuple-element.180), kind=kOutput, calls=%fused_computation.1.clone.1 | convolution fusion | flops 541063168 | bytes 18096640 | tf_op jit(solution)/shard_map/while/body/eval_jaxpr/qhgd,khd->hgqk/dot_general | solution.py:109
  162.5 7.6 %fusion.55 = f32[256,4,2,64]{0,3,2,1:T(8,128)S(1)} fusion(f32[4,2048,256,2]{2,1,3,0:T(8,128)} %get-tuple-element.169, f32[4,2,256]{2,1,0:T(2,128)S(1)} %get-tuple-element.190, bf16[2,2048,4,64]{1,3,2,0:T(8,128)(2,1)} %get-tuple-element.195, s32[]{:T(128)} %get-tuple-element.180, f32[256,4,2,64]{0,3,2,1:T(8,128)S(1)} %get-tuple-element.183, ...), kind=kOutput, calls=%fused_computation.8.clone.1 | convolution fusion | flops 545652736 | bytes 18891264 | tf_op jit(solution)/shard_map/while/body/eval_jaxpr/hgqk,khd->qhgd/dot_general | solution.py:116
  170.1 8.0 %fusion.53 = f32[4,2,256]{2,1,0:T(2,128)S(1)} fusion(f32[4,2048,256,2]{2,1,3,0:T(8,128)} %get-tuple-element.169, f32[4,2,256]{2,1,0:T(2,128)S(1)} %get-tuple-element.190), kind=kLoop, calls=%fused_computation.4.clone.1 | loop fusion | flops 8386560 | bytes 16793600 | tf_op jit(solution)/shard_map/while/body/eval_jaxpr/reduce_sum | solution.py:115
  178.1 9.3 %bitcast_reduce_fusion.2 = (f32[4,2,256]{2,1,0:T(2,128)S(1)}, f32[4,2048,256,2]{2,1,3,0:T(8,128)}) fusion(bf16[256,4,2,64]{0,3,2,1:T(8,128)(2,1)S(1)} %get-tuple-element.194, bf16[2,2048,4,64]{1,3,2,0:T(8,128)(2,1)} %get-tuple-element.193, s32[]{:T(128)} %get-tuple-element.180), kind=kOutput, calls=%fused_computation.1.clone.1 | convolution fusion | flops 541063168 | bytes 18096640 | tf_op jit(solution)/shard_map/while/body/eval_jaxpr/qhgd,khd->hgqk/dot_general | solution.py:109
  187.5 7.6 %fusion.55 = f32[256,4,2,64]{0,3,2,1:T(8,128)S(1)} fusion(f32[4,2048,256,2]{2,1,3,0:T(8,128)} %get-tuple-element.169, f32[4,2,256]{2,1,0:T(2,128)S(1)} %get-tuple-element.190, bf16[2,2048,4,64]{1,3,2,0:T(8,128)(2,1)} %get-tuple-element.195, s32[]{:T(128)} %get-tuple-element.180, f32[256,4,2,64]{0,3,2,1:T(8,128)S(1)} %get-tuple-element.183, ...), kind=kOutput, calls=%fused_computation.8.clone.1 | convolution fusion | flops 545652736 | bytes 18891264 | tf_op jit(solution)/shard_map/while/body/eval_jaxpr/hgqk,khd->qhgd/dot_general | solution.py:116
  195.0 8.0 %fusion.53 = f32[4,2,256]{2,1,0:T(2,128)S(1)} fusion(f32[4,2048,256,2]{2,1,3,0:T(8,128)} %get-tuple-element.169, f32[4,2,256]{2,1,0:T(2,128)S(1)} %get-tuple-element.190), kind=kLoop, calls=%fused_computation.4.clone.1 | loop fusion | flops 8386560 | bytes 16793600 | tf_op jit(solution)/shard_map/while/body/eval_jaxpr/reduce_sum | solution.py:115
  203.1 1.7 convolution_convert_fusion.1
  204.9 0.0 all-reduce.3.cloned.1.call-update
  204.9 0.0 all-gather.11.cloned.1.call-start
  204.9 0.5 all-gather.11.cloned.1.call-update
  205.5 0.0 all-gather.9.cloned.1.call-start
  205.5 0.5 all-gather.9.cloned.1.call-update
  206.1 0.0 copy-start.2
  206.1 0.0 copy-start.3
  206.1 0.2 reduce-scatter.2.cloned.1.call-start
  206.3 17.0 %all-reduce.3.cloned.1.call-done = bf16[256,2048]{1,0:T(8,128)(2,1)} async-done(((bf16[256,2048]{1,0:T(8,128)(2,1)}), bf16[256,2048]{1,0:T(8,128)(2,1)}) %all-reduce.3.cloned.1.call-update) | async-done | bytes 1048592 | tf_op jit(solution)/shard_map/psum | solution.py:135
  223.3 2.0 fusion.24
  225.4 1.8 multiply_reduce_fusion
  227.2 0.0 copy-done.3
  227.2 2.8 add_convert_fusion
  230.0 246.2 %all-gather.11.cloned.1.call-done = bf16[4096,2048]{1,0:T(8,128)(2,1)} async-done(((bf16[4096,128]{1,0:T(8,128)(2,1)}), bf16[4096,2048]{1,0:T(8,128)(2,1)}) %all-gather.11.cloned.1.call-update) | async-done | bytes 16777232 | tf_op jit(solution)/shard_map/all_gather | solution.py:148
  476.2 191.8 %all-gather.9.cloned.1.call-done = bf16[2048,4096]{1,0:T(8,128)(2,1)} async-done(((bf16[128,4096]{1,0:T(8,128)(2,1)}), bf16[2048,4096]{1,0:T(8,128)(2,1)}) %all-gather.9.cloned.1.call-update) | async-done | bytes 16777232 | tf_op jit(solution)/shard_map/all_gather | solution.py:142
  668.0 16.5 %convolution_convert_fusion = bf16[256,2048]{1,0:T(8,128)(2,1)} fusion(bf16[4096,2048]{1,0:T(8,128)(2,1)} %all-gather.11.cloned.1.call-done, bf16[256,2048]{1,0:T(8,128)(2,1)} %add_convert_fusion, bf16[2048,4096]{1,0:T(8,128)(2,1)} %all-gather.9.cloned.1.call-done), kind=kOutput, calls=%fused_computation.26 | convolution fusion | flops 8593604608 | bytes 35651584 | tf_op jit(solution)/shard_map/dot_general | solution.py:146
  684.5 0.0 reduce-scatter.2.cloned.1.call-update
  684.6 6.7 reduce-scatter.2.cloned.1.call-done
  691.2 1.5 fusion.25
  692.8 2.5 all-reduce
  695.3 2.3 add_convert_fusion.1
  (33 shorter events, 0.4 us)
Async XLA Ops:
  6.5 196.6 %copy-start = (bf16[512,2048]{1,0:T(8,128)(2,1)S(1)}, bf16[512,2048]{1,0:T(8,128)(2,1)}, u32[]{:S(2)}) copy-start(bf16[512,2048]{1,0:T(8,128)(2,1)} %param.20) | copy-start | bytes 6291460
  6.5 4.9 copy-start.6
  6.5 71.0 %all-gather.5.cloned.1.call-start = ((), (), s32[]{:S(2)}) async-start(), calls=%async_computation.1 | async-start | bytes 2228224 | tf_op jit(solution)/shard_map/all_gather | solution.py:100
  9.5 129.6 %all-gather.7.cloned.1.call-start = ((), (), s32[]{:S(2)}) async-start(), calls=%async_computation.2 | async-start | bytes 2228224 | tf_op jit(solution)/shard_map/all_gather | solution.py:101
  10.2 213.1 %all-reduce.3.cloned.1.call-start = ((), (), s32[]{:S(2)}) async-start(), calls=%async_computation.3 | async-start | bytes 2097152 | tf_op jit(solution)/shard_map/psum | solution.py:135
  204.9 271.3 %all-gather.11.cloned.1.call-start = ((), (), s32[]{:S(2)}) async-start(), calls=%async_computation.5 | async-start | bytes 17825792 | tf_op jit(solution)/shard_map/all_gather | solution.py:148
  205.5 462.5 %all-gather.9.cloned.1.call-start = ((), (), s32[]{:S(2)}) async-start(), calls=%async_computation.4 | async-start | bytes 17825792 | tf_op jit(solution)/shard_map/all_gather | solution.py:142
  206.1 21.1 %copy-start.2 = (f32[2048]{0:T(1024)S(1)}, f32[2048]{0:T(1024)}, u32[]{:S(2)}) copy-start(f32[2048]{0:T(1024)} %param.23) | copy-start | bytes 24580
  206.1 21.1 %copy-start.3 = (f32[2048]{0:T(1024)S(1)}, f32[2048]{0:T(1024)}, u32[]{:S(2)}) copy-start(f32[2048]{0:T(1024)} %param.22) | copy-start | bytes 24580
  206.1 485.2 %reduce-scatter.2.cloned.1.call-start = ((), (), s32[]{:S(2)}) async-start(), calls=%async_computation.6 | async-start | bytes 1572864 | tf_op jit(solution)/shard_map/reduce_scatter | solution.py:151
  223.3 2.1 copy-start.1
  230.0 454.5 %copy-start.4 = (f32[2048]{0:T(1024)S(1)}, f32[2048]{0:T(1024)}, u32[]{:S(2)}) copy-start(f32[2048]{0:T(1024)} %param.26) | copy-start | bytes 24580
  230.0 454.5 %copy-start.5 = (f32[2048]{0:T(1024)S(1)}, f32[2048]{0:T(1024)}, u32[]{:S(2)}) copy-start(f32[2048]{0:T(1024)} %param.27) | copy-start | bytes 24580
Sparse Core Ops, SparseCore 0:
  10.1 67.4 all-gather.4
  80.3 58.7 all-gather.6
  205.0 18.2 all-reduce.2
  225.8 250.2 all-gather.10
  478.8 189.1 all-gather.8
  684.6 6.5 reduce-scatter.1
where the time goes:
time: 705 us; the launch traced here: 704 us
  waiting for transfers between devices  583 us (83%)
  matrix products  52 us (7%)
  other arithmetic  28.7 us (4%)
  local copies, waits for them, and re-layouts  24.6 us (3%)
  between operations  13.7 us (2%)
    all_gather x1, waiting for transfers between devices, local(): lax.all_gather(down_weight, 'sp', axis=1, tiled=True)  246 us
    all_gather x1, waiting for transfers between devices, local(): lax.all_gather(up_weight, 'sp', axis=0, tiled=True)  192 us
    all_gather x1, waiting for transfers between devices, local(): key_piece = lax.all_gather(k_sent, 'sp', axis=0, tiled=True)  65.8 us
    all_gather x1, waiting for transfers between devices, local(): value_piece = lax.all_gather(values, 'sp', axis=0, tiled=True)  53.3 us
    dot_general x2, matrix products, advance(): jnp.einsum('qhgd,khd->hgqk', q_grouped, blocks[0], preferred_element_type...  18.7 us
    psum x1, waiting for transfers between devices, local(): lax.psum(partial_value.astype(jnp.bfloat16), 'tp').astype(jnp.float32)  17 us
    dot_general x1, matrix products, local(): jnp.dot(hidden, lax.all_gather(down_weight, 'sp', axis=1, tiled=True), pr...  16.5 us
    reduce_sum x2, other arithmetic, advance(): totals = totals * factor + jnp.sum(weights, -1)  16 us
  transfers between devices with their start and end apart: 6, of which 6 were waited for; matrix products, arithmetic and copies ran while one was open for 2% of the time, Pallas kernels for 0%

commit v1 on v0

--- a/solution.py
+++ b/solution.py
@@ -145,7 +145,7 @@
     hidden = jnp.square(jnp.maximum(up_acts, 0.0)).astype(jnp.bfloat16)
     partial_ffn = jnp.dot(
         hidden,
-        lax.all_gather(down_weight, "sp", axis=1, tiled=True),
+        jnp.concatenate(lax.all_gather(down_weight, "sp"), axis=1),
         preferred_element_type=jnp.float32,
     )
     ffn_cols = lax.psum_scatter(

time: 705 us -> 647 us (0.918)
  waiting for transfers between devices: 583 us -> 506 us
  local copies, waits for them, and re-layouts: 24.6 us -> 45.6 us
    all_gather x1, waiting for transfers between devices: 246 us -> 191 us  [local(): lax.all_gather(down_weight, 'sp')]
    all_gather x1, waiting for transfers between devices: 192 us -> 171 us  [local(): lax.all_gather(up_weight, 'sp', axis=0, tiled=True)]
    reshape x0 -> x1, local copies, waits for them, and re-layouts: none -> 21 us  [local(): jnp.concatenate(lax.all_gather(down_weight, 'sp'), axis=1)]
  transfers between devices with their start and end apart: 6 -> 6, of which waited for: 6 -> 6; matrix products, arithmetic and copies ran while one was open for 2% -> 5% of each run, Pallas kernels for 0% -> 0%
where the time goes in v1:
time: 647 us; the launch traced here: 646 us
  waiting for transfers between devices  506 us (78%)
  matrix products  51.7 us (8%)
  local copies, waits for them, and re-layouts  45.6 us (7%)
  other arithmetic  25.6 us (4%)
  between operations  13.7 us (2%)
    all_gather x1, waiting for transfers between devices, local(): lax.all_gather(down_weight, 'sp')  191 us
    all_gather x1, waiting for transfers between devices, local(): lax.all_gather(up_weight, 'sp', axis=0, tiled=True)  171 us
    all_gather x1, waiting for transfers between devices, local(): key_piece = lax.all_gather(k_sent, 'sp', axis=0, tiled=True)  65.8 us
    all_gather x1, waiting for transfers between devices, local(): value_piece = lax.all_gather(values, 'sp', axis=0, tiled=True)  53.3 us
    reshape x1, local copies, waits for them, and re-layouts, local(): jnp.concatenate(lax.all_gather(down_weight, 'sp'), axis=1)  21 us
    dot_general x2, matrix products, advance(): jnp.einsum('qhgd,khd->hgqk', q_grouped, blocks[0], preferred_element_type...  18.7 us
    psum x1, waiting for transfers between devices, local(): lax.psum(partial_value.astype(jnp.bfloat16), 'tp').astype(jnp.float32)  17 us
    dot_general x1, matrix products, local(): jnp.dot(hidden, jnp.concatenate(lax.all_gather(down_weight, 'sp'), axis=1...  16.2 us
  transfers between devices with their start and end apart: 6, of which 6 were waited for; matrix products, arithmetic and copies ran while one was open for 5% of the time, Pallas kernels for 0%

profile of v1, /device:TPU:0, one launch (start us, length us, event | category | flops | bytes accessed | tf_op | source)
XLA Modules:
  0.0 645.8 jit_solution(16319847087977932795)
XLA Ops:
  6.6 1.1 copy.27
  7.8 0.7 fusion.30
  8.5 0.2 multiply_cosine_fusion.1
  8.8 0.7 pad_maximum_fusion
  9.4 0.0 all-gather.6.cloned.1.call-update
  9.5 0.0 all-gather.8.cloned.1.call-start
  9.5 0.7 all-gather.8.cloned.1.call-update
  10.2 0.0 all-reduce.3.cloned.1.call-start
  10.3 1.1 copy.28
  11.4 0.1 fusion.26
  11.5 0.1 fusion.27
  11.6 0.1 multiply_subtract_fusion.1
  11.7 65.8 %all-gather.6.cloned.1.call-done = bf16[4096,256]{0,1:T(8,128)(2,1)} async-done(((bf16[256,256]{0,1:T(8,128)(2,1)}), bf16[4096,256]{0,1:T(8,128)(2,1)}) %all-gather.6.cloned.1.call-update) | async-done | bytes 2097168 | tf_op jit(solution)/shard_map/all_gather | solution.py:100
  77.5 4.5 reshape.207
  82.0 3.8 copy.30
  85.8 53.3 %all-gather.8.cloned.1.call-done = bf16[4096,256]{1,0:T(8,128)(2,1)} async-done(((bf16[256,256]{1,0:T(8,128)(2,1)}), bf16[4096,256]{1,0:T(8,128)(2,1)}) %all-gather.8.cloned.1.call-update) | async-done | bytes 2097168 | tf_op jit(solution)/shard_map/all_gather | solution.py:101
  139.1 7.1 %reshape.216 = bf16[2,2048,4,64]{3,2,1,0:T(4,128)(2,1)} reshape(bf16[4096,256]{1,0:T(8,128)(2,1)} %all-gather.8.cloned.1.call-done) | data formatting | bytes 4194304 | tf_op jit(solution)/shard_map/reshape | solution.py:105
  146.2 7.0 %copy.31 = bf16[2,2048,4,64]{1,3,2,0:T(8,128)(2,1)} copy(bf16[2,2048,4,64]{3,2,1,0:T(4,128)(2,1)} %reshape.216) | data formatting | bytes 4194304
  153.1 49.9 %while.15 = (s32[]{:T(128)}, f32[4,2,256]{2,1,0:T(2,128)S(1)}, f32[4,2,256]{2,1,0:T(2,128)S(1)}, f32[256,4,2,64]{0,3,2,1:T(8,128)S(1)}, bf16[2,2048,4,64]{1,3,2,...) while((s32[]{:T(128)}, f32[4,2,256]{2,1,0:T(2,128)S(1)}, ...), condition=%wide.region_5.6_spmd.clone, body=%wide.region_2.5_spmd.clone.sunk | while | flops 1095118848 | bytes 53871716 | solution.py:125
  153.1 9.3 %bitcast_reduce_fusion.2 = (f32[4,2,256]{2,1,0:T(2,128)S(1)}, f32[4,2048,256,2]{2,1,3,0:T(8,128)}) fusion(bf16[256,4,2,64]{0,3,2,1:T(8,128)(2,1)S(1)} %get-tuple-element.201, bf16[2,2048,4,64]{1,3,2,0:T(8,128)(2,1)} %get-tuple-element.200, s32[]{:T(128)} %get-tuple-element.187), kind=kOutput, calls=%fused_computation.1.clone.1 | convolution fusion | flops 541063168 | bytes 18096640 | tf_op jit(solution)/shard_map/while/body/eval_jaxpr/qhgd,khd->hgqk/dot_general | solution.py:109
  162.5 7.6 %fusion.55 = f32[256,4,2,64]{0,3,2,1:T(8,128)S(1)} fusion(f32[4,2048,256,2]{2,1,3,0:T(8,128)} %get-tuple-element.176, f32[4,2,256]{2,1,0:T(2,128)S(1)} %get-tuple-element.197, bf16[2,2048,4,64]{1,3,2,0:T(8,128)(2,1)} %get-tuple-element.202, s32[]{:T(128)} %get-tuple-element.187, f32[256,4,2,64]{0,3,2,1:T(8,128)S(1)} %get-tuple-element.190, ...), kind=kOutput, calls=%fused_computation.8.clone.1 | convolution fusion | flops 545652736 | bytes 18891264 | tf_op jit(solution)/shard_map/while/body/eval_jaxpr/hgqk,khd->qhgd/dot_general | solution.py:116
  170.1 8.0 %fusion.53 = f32[4,2,256]{2,1,0:T(2,128)S(1)} fusion(f32[4,2048,256,2]{2,1,3,0:T(8,128)} %get-tuple-element.176, f32[4,2,256]{2,1,0:T(2,128)S(1)} %get-tuple-element.197), kind=kLoop, calls=%fused_computation.4.clone.1 | loop fusion | flops 8386560 | bytes 16793600 | tf_op jit(solution)/shard_map/while/body/eval_jaxpr/reduce_sum | solution.py:115
  178.1 9.3 %bitcast_reduce_fusion.2 = (f32[4,2,256]{2,1,0:T(2,128)S(1)}, f32[4,2048,256,2]{2,1,3,0:T(8,128)}) fusion(bf16[256,4,2,64]{0,3,2,1:T(8,128)(2,1)S(1)} %get-tuple-element.201, bf16[2,2048,4,64]{1,3,2,0:T(8,128)(2,1)} %get-tuple-element.200, s32[]{:T(128)} %get-tuple-element.187), kind=kOutput, calls=%fused_computation.1.clone.1 | convolution fusion | flops 541063168 | bytes 18096640 | tf_op jit(solution)/shard_map/while/body/eval_jaxpr/qhgd,khd->hgqk/dot_general | solution.py:109
  187.5 7.6 %fusion.55 = f32[256,4,2,64]{0,3,2,1:T(8,128)S(1)} fusion(f32[4,2048,256,2]{2,1,3,0:T(8,128)} %get-tuple-element.176, f32[4,2,256]{2,1,0:T(2,128)S(1)} %get-tuple-element.197, bf16[2,2048,4,64]{1,3,2,0:T(8,128)(2,1)} %get-tuple-element.202, s32[]{:T(128)} %get-tuple-element.187, f32[256,4,2,64]{0,3,2,1:T(8,128)S(1)} %get-tuple-element.190, ...), kind=kOutput, calls=%fused_computation.8.clone.1 | convolution fusion | flops 545652736 | bytes 18891264 | tf_op jit(solution)/shard_map/while/body/eval_jaxpr/hgqk,khd->qhgd/dot_general | solution.py:116
  195.0 8.0 %fusion.53 = f32[4,2,256]{2,1,0:T(2,128)S(1)} fusion(f32[4,2048,256,2]{2,1,3,0:T(8,128)} %get-tuple-element.176, f32[4,2,256]{2,1,0:T(2,128)S(1)} %get-tuple-element.197), kind=kLoop, calls=%fused_computation.4.clone.1 | loop fusion | flops 8386560 | bytes 16793600 | tf_op jit(solution)/shard_map/while/body/eval_jaxpr/reduce_sum | solution.py:115
  203.1 1.8 convolution_convert_fusion.1
  204.9 0.0 all-reduce.3.cloned.1.call-update
  204.9 0.0 all-gather.12.cloned.1.call-start
  205.0 0.5 all-gather.12.cloned.1.call-update
  205.5 0.0 all-gather.10.cloned.1.call-start
  205.6 0.5 all-gather.10.cloned.1.call-update
  206.1 0.0 copy-start.4
  206.1 0.0 copy-start.5
  206.1 0.2 reduce-scatter.2.cloned.1.call-start
  206.3 17.0 %all-reduce.3.cloned.1.call-done = bf16[256,2048]{1,0:T(8,128)(2,1)} async-done(((bf16[256,2048]{1,0:T(8,128)(2,1)}), bf16[256,2048]{1,0:T(8,128)(2,1)}) %all-reduce.3.cloned.1.call-update) | async-done | bytes 1048592 | tf_op jit(solution)/shard_map/psum | solution.py:135
  223.3 1.7 fusion.24
  225.1 0.6 multiply_reduce_fusion
  225.7 0.0 copy-done.5
  225.7 1.6 add_convert_fusion
  227.3 190.9 %all-gather.12.cloned.1.call-done = bf16[65536,128]{1,0:T(8,128)(2,1)} async-done(((bf16[4096,128]{1,0:T(8,128)(2,1)}), bf16[65536,128]{1,0:T(8,128)(2,1)}) %all-gather.12.cloned.1.call-update) | async-done | bytes 16777232 | tf_op jit(solution)/shard_map/all_gather | solution.py:148
  418.2 21.0 %copy.32 = bf16[4096,16,128]{0,2,1:T(8,128)(2,1)} copy(bf16[4096,16,128]{2,0,1:T(8,128)(2,1)} %bitcast.77) | data formatting | bytes 33554432 | tf_op jit(solution)/shard_map/reshape | solution.py:148
  439.1 170.9 %all-gather.10.cloned.1.call-done = bf16[2048,4096]{1,0:T(8,128)(2,1)} async-done(((bf16[128,4096]{1,0:T(8,128)(2,1)}), bf16[2048,4096]{1,0:T(8,128)(2,1)}) %all-gather.10.cloned.1.call-update) | async-done | bytes 16777232 | tf_op jit(solution)/shard_map/all_gather | solution.py:142
  610.0 16.2 %convolution_convert_fusion = bf16[256,2048]{1,0:T(8,128)(2,1)} fusion(bf16[4096,2048]{0,1:T(8,128)(2,1)} %bitcast.78, bf16[256,2048]{1,0:T(8,128)(2,1)S(1)} %copy-done.3, bf16[2048,4096]{1,0:T(8,128)(2,1)} %all-gather.10.cloned.1.call-done), kind=kOutput, calls=%fused_computation.26 | convolution fusion | flops 8593604608 | bytes 35651584 | tf_op jit(solution)/shard_map/dot_general | solution.py:146
  626.2 0.0 reduce-scatter.2.cloned.1.call-update
  626.3 6.7 %reduce-scatter.2.cloned.1.call-done = bf16[256,1024]{1,0:T(8,128)(2,1)} async-done(((bf16[256,2048]{1,0:T(8,128)(2,1)}), bf16[256,1024]{1,0:T(8,128)(2,1)}) %reduce-scatter.2.cloned.1.call-update) | async-done | bytes 524304 | tf_op jit(solution)/shard_map/reduce_scatter | solution.py:151
  632.9 1.4 fusion.25
  634.3 2.5 all-reduce
  636.8 2.1 add_convert_fusion.1
  (38 shorter events, 0.4 us)
Async XLA Ops:
  6.5 196.6 %copy-start = (bf16[512,2048]{1,0:T(8,128)(2,1)S(1)}, bf16[512,2048]{1,0:T(8,128)(2,1)}, u32[]{:S(2)}) copy-start(bf16[512,2048]{1,0:T(8,128)(2,1)} %param.20) | copy-start | bytes 6291460
  6.5 4.9 copy-start.8
  6.5 71.0 %all-gather.6.cloned.1.call-start = ((), (), s32[]{:S(2)}) async-start(), calls=%async_computation.1 | async-start | bytes 2228224 | tf_op jit(solution)/shard_map/all_gather | solution.py:100
  9.5 129.6 %all-gather.8.cloned.1.call-start = ((), (), s32[]{:S(2)}) async-start(), calls=%async_computation.2 | async-start | bytes 2228224 | tf_op jit(solution)/shard_map/all_gather | solution.py:101
  10.2 213.1 %all-reduce.3.cloned.1.call-start = ((), (), s32[]{:S(2)}) async-start(), calls=%async_computation.3 | async-start | bytes 2097152 | tf_op jit(solution)/shard_map/psum | solution.py:135
  204.9 18.4 %copy-start.1 = (bf16[256,2048]{1,0:T(8,128)(2,1)S(1)}, bf16[256,2048]{1,0:T(8,128)(2,1)}, u32[]{:S(2)}) copy-start(bf16[256,2048]{1,0:T(8,128)(2,1)} %param.21) | copy-start | bytes 3145732
  204.9 213.2 %all-gather.12.cloned.1.call-start = ((), (), s32[]{:S(2)}) async-start(), calls=%async_computation.6 | async-start | bytes 17825792 | tf_op jit(solution)/shard_map/all_gather | solution.py:148
  205.5 404.5 %all-gather.10.cloned.1.call-start = ((), (), s32[]{:S(2)}) async-start(), calls=%async_computation.4 | async-start | bytes 17825792 | tf_op jit(solution)/shard_map/all_gather | solution.py:142
  206.1 19.6 %copy-start.4 = (f32[2048]{0:T(1024)S(1)}, f32[2048]{0:T(1024)}, u32[]{:S(2)}) copy-start(f32[2048]{0:T(1024)} %param.23) | copy-start | bytes 24580
  206.1 19.5 %copy-start.5 = (f32[2048]{0:T(1024)S(1)}, f32[2048]{0:T(1024)}, u32[]{:S(2)}) copy-start(f32[2048]{0:T(1024)} %param.22) | copy-start | bytes 24580
  206.1 426.8 %reduce-scatter.2.cloned.1.call-start = ((), (), s32[]{:S(2)}) async-start(), calls=%async_computation.5 | async-start | bytes 1572864 | tf_op jit(solution)/shard_map/reduce_scatter | solution.py:151
  223.3 1.7 copy-start.2
  418.2 191.8 %copy-start.3 = (bf16[256,2048]{1,0:T(8,128)(2,1)S(1)}, bf16[256,2048]{1,0:T(8,128)(2,1)}, u32[]{:S(2)}) copy-start(bf16[256,2048]{1,0:T(8,128)(2,1)} %add_convert_fusion) | copy-start | bytes 3145732
  610.0 16.2 %copy-start.6 = (f32[2048]{0:T(1024)S(1)}, f32[2048]{0:T(1024)}, u32[]{:S(2)}) copy-start(f32[2048]{0:T(1024)} %param.26) | copy-start | bytes 24580
  610.0 16.2 %copy-start.7 = (f32[2048]{0:T(1024)S(1)}, f32[2048]{0:T(1024)}, u32[]{:S(2)}) copy-start(f32[2048]{0:T(1024)} %param.27) | copy-start | bytes 24580
Sparse Core Ops, SparseCore 0:
  10.1 67.4 all-gather.5
  80.3 58.7 all-gather.7
  205.0 18.2 all-reduce.2
  225.9 192.1 all-gather.11
  420.8 189.1 all-gather.9
  626.3 6.5 reduce-scatter.1
